TPU v7x, 32 devices: a whole 2x2x4 slice. The times are simulated.
32 devices in a mesh: dp: 4 (over y, x), kv: 4 (over z), tp: 2 (over core).
Axes of the slice: x: 2, y: 2, z: 4, core: 2. Of those that a mesh axis runs over, the one named last changes fastest.
Arguments:
- tokens: bfloat16 [32, 4096], P('dp', ('kv', 'tp')), may hold values from -7 to 7
- mix_gain: float32 [4096], replicated, may hold values from 0.1 to 1.9
- query_weight: bfloat16 [16, 128, 4096], P('tp', 'kv'), may hold values from -0.09375 to 0.09375
- forget_weight: bfloat16 [16, 128, 4096], P('tp', 'kv'), may hold values from -0.09375 to 0.09375
- value_weight: bfloat16 [16, 128, 4096], P('tp', 'kv'), may hold values from -0.09375 to 0.09375
- gate_weight: bfloat16 [16, 128, 4096], P('tp', 'kv'), may hold values from -0.09375 to 0.09375
- lower_bound: float32 [16, 128], P('tp'), may hold values from 0.02 to 0.9
- recurrent_state: float32 [32, 16, 128, 128], P(('dp', 'kv'), 'tp'), may hold values from -3 to 3
- head_gain: float32 [16, 128], P('tp'), may hold values from 0.1 to 1.9
- out_weight: bfloat16 [16, 128, 4096], P(None, None, ('kv', 'tp')), may hold values from -0.125 to 0.125
- mlp_gain: float32 [4096], replicated, may hold values from 0.1 to 1.9
- up_weight: bfloat16 [4096, 16384], P(None, ('kv', 'tp')), may hold values from -0.09375 to 0.09375
- down_weight: bfloat16 [16384, 4096], P(('kv', 'tp')), may hold values from -0.0625 to 0.0625
Outputs:
- layer_output: bfloat16 [32, 4096], P('dp', ('kv', 'tp'))
- next_state: float32 [32, 16, 128, 128], P(('dp', 'kv'), 'tp')
All inputs are finite; a program needn't handle non-finite values.
Results may differ from a plain program's by a relative error of at most 0.0072.
Values may be sent and summed in bfloat16 or wider, within the bound.
A program may use at most 128 MiB of HBM per device.

v0:
```python
import jax
import jax.numpy as jnp
from jax import lax
from jax.sharding import PartitionSpec as P

epsilon = 1e-06


def normed_rows(row_block, gain_vector):
    whole_rows = lax.all_gather(row_block, ("kv", "tp"), axis=1, tiled=True).astype(jnp.float32)
    inv_root = lax.rsqrt(jnp.mean(whole_rows * whole_rows, axis=1, keepdims=True) + epsilon)
    result_rows = (whole_rows * inv_root * gain_vector).astype(jnp.bfloat16)
    return result_rows


def local(
    tokens,
    mix_gain,
    query_weight,
    forget_weight,
    value_weight,
    gate_weight,
    lower_bound,
    recurrent_state,
    head_gain,
    out_weight,
    mlp_gain,
    up_weight,
    down_weight,
):
    normed = normed_rows(tokens, mix_gain)
    local_heads, local_chan, width = query_weight.shape
    stacked = jnp.stack((query_weight, forget_weight, value_weight, gate_weight), axis=0).reshape(
        -1, width
    )
    product = lax.dot_general(
        normed, stacked, (((1,), (1,)), ((), ())), preferred_element_type=jnp.float32
    ).astype(jnp.bfloat16)
    product = product.reshape(normed.shape[0], 4, local_heads, local_chan)
    pre_query, pre_forget, value_rows, pre_gate = (
        lax.all_to_all(product[:, 0], "kv", split_axis=0, concat_axis=2, tiled=True),
        lax.all_to_all(product[:, 1], "kv", split_axis=0, concat_axis=2, tiled=True),
        lax.all_to_all(product[:, 2], "kv", split_axis=0, concat_axis=2, tiled=True),
        lax.all_to_all(product[:, 3], "kv", split_axis=0, concat_axis=2, tiled=True),
    )
    log_forget = jnp.logaddexp(
        jnp.log(lower_bound),
        jnp.log1p(-lower_bound) + jax.nn.log_sigmoid(pre_forget.astype(jnp.float32)),
    )
    key_rows = -jnp.expm1(log_forget)
    next_state = (
        jnp.exp(log_forget)[:, :, :, None] * recurrent_state
        + key_rows[:, :, :, None] * value_rows.astype(jnp.float32)[:, :, None, :]
    )
    query_act = jax.nn.silu(pre_query.astype(jnp.float32))
    readout = jnp.einsum("bhk,bhkv->bhv", query_act, next_state, precision=lax.Precision.HIGHEST)
    inv_head = lax.rsqrt(jnp.mean(readout * readout, axis=2, keepdims=True) + epsilon)
    mixed_heads = (
        readout * inv_head * head_gain * jax.nn.silu(pre_gate.astype(jnp.float32))
    ).astype(jnp.bfloat16)
    all_heads = lax.all_gather(mixed_heads, "tp", axis=1, tiled=True)
    flat_mixed = all_heads.reshape(all_heads.shape[0], -1)
    out_matrix = out_weight.reshape(-1, out_weight.shape[2])
    projected = jnp.dot(
        lax.all_gather(flat_mixed, "kv", axis=0, tiled=True),
        out_matrix,
        preferred_element_type=jnp.float32,
    )
    residual = lax.optimization_barrier(
        (tokens.astype(jnp.float32) + projected).astype(jnp.bfloat16)
    )
    normed_mlp = normed_rows(residual, mlp_gain)
    hidden = jnp.square(
        jax.nn.relu(jnp.dot(normed_mlp, up_weight, preferred_element_type=jnp.float32))
    ).astype(jnp.bfloat16)
    summed = lax.psum_scatter(
        jnp.dot(hidden, down_weight, preferred_element_type=jnp.float32),
        ("kv", "tp"),
        scatter_dimension=1,
        tiled=True,
    )
    layer_output = (residual.astype(jnp.float32) + summed).astype(jnp.bfloat16)
    return (layer_output, next_state)


def solution(mesh):
    placed = (
        P("dp", ("kv", "tp")),
        P(),
        P("tp", "kv", None),
        P("tp", "kv", None),
        P("tp", "kv", None),
        P("tp", "kv", None),
        P("tp", None),
        P(("dp", "kv"), "tp", None, None),
        P("tp", None),
        P(None, None, ("kv", "tp")),
        P(),
        P(None, ("kv", "tp")),
        P(("kv", "tp"), None),
    )
    return jax.shard_map(
        local,
        mesh=mesh,
        in_specs=placed,
        out_specs=(P("dp", ("kv", "tp")), P(("dp", "kv"), "tp", None, None)),
        check_vma=False,
    )
```

profile of v0, /device:TPU:0, one launch (start us, length us, event | category | flops | bytes accessed | tf_op | source)
XLA Modules:
  0.0 148.9 jit_solution(8380039019351915380)
XLA Ops:
  7.2 0.0 copy-start
  7.2 16.0 %all_gather.12 = bf16[8,4096]{1,0:T(8,128)(2,1)S(1)} all-gather(bf16[8,512]{1,0:T(8,128)(2,1)} %param.13), channel_id=1, replica_groups=mesh['dp'=4,'kv'=4,'tp'=2] {'kv','tp'}, dimensions={1}, use_global_device_ids=true | all-gather | bytes 73728 | tf_op jit(solution)/shard_map/all_gather | solution.py:10
  23.2 0.1 fusion.4
  23.4 4.4 %pad_maximum_fusion = bf16[4,8,32,4096]{3,2,1,0:T(8,128)(2,1)S(1)} fusion(bf16[1,8,32,4096]{3,2,1,0:T(8,128)(2,1)} %bitcast.47, bf16[1,8,32,4096]{3,2,1,0:T(8,128)(2,1)} %bitcast.48, bf16[1,8,32,4096]{3,2,1,0:T(8,128)(2,1)} %bitcast.49, bf16[1,8,32,4096]{3,2,1,0:T(8,128)(2,1)} %bitcast.50), kind=kLoop, calls=%fused_computation | loop fusion | flops 12582912 | bytes 16777216 | tf_op jit(solution)/shard_map/stack | solution.py:33
  27.7 0.0 copy-start.5
  27.8 0.0 copy-start.6
  27.8 0.0 copy-start.2
  27.8 0.0 copy-start.4
  27.8 2.3 %convolution_convert_fusion = bf16[8,1024]{1,0:T(8,128)(2,1)S(1)} fusion(bf16[1024,4096]{1,0:T(8,128)(2,1)S(1)} %bitcast.46, bf16[8,4096]{1,0:T(8,128)(2,1)S(1)} %all_gather.12, f32[4096]{0:T(1024)S(1)} %copy-done.3, f32[8]{0:T(128)S(1)} %add_rsqrt_fusion.2), kind=kOutput, calls=%fused_computation.4 | convolution fusion | flops 67248128 | bytes 8486944 | tf_op jit(solution)/shard_map/dot_general | solution.py:36
  30.1 0.1 reshape.99
  30.2 0.7 reshape.119
  30.9 4.6 %all-to-all-start.1 = ((bf16[4,2,256]{2,1,0:T(2,128)(2,1)}), bf16[4,2,256]{2,1,0:T(2,128)(2,1)S(1)}, u32[]{:S(2)}, u32[]{:S(2)}) async-start(bf16[4,2,256]{2,1,0:T(2,128)(2,1)} %reshape.119), calls=%async_computation.1 | async-start | bytes 8192 | tf_op jit(solution)/shard_map/all_to_all | solution.py:42
  35.6 0.7 reshape.117
  36.2 0.7 reshape.115
  36.9 0.7 reshape.113
  37.6 3.5 %all-to-all-done.1 = bf16[4,2,256]{2,1,0:T(2,128)(2,1)S(1)} async-done(((bf16[4,2,256]{2,1,0:T(2,128)(2,1)}), bf16[4,2,256]{2,1,0:T(2,128)(2,1)S(1)}, u32[]{:S(2)}, u32[]{:S(2)}) %all-to-all-start.1) | async-done | bytes 4128 | tf_op jit(solution)/shard_map/all_to_all | solution.py:42
  41.1 3.2 %all-to-all-start.2 = ((bf16[4,2,256]{2,1,0:T(2,128)(2,1)}), bf16[4,2,256]{2,1,0:T(2,128)(2,1)S(1)}, u32[]{:S(2)}, u32[]{:S(2)}) async-start(bf16[4,2,256]{2,1,0:T(2,128)(2,1)} %reshape.117), calls=%async_computation.2 | async-start | bytes 8192 | tf_op jit(solution)/shard_map/all_to_all | solution.py:43
  44.3 0.1 reshape.120
  44.4 5.4 %all-to-all-done.2 = bf16[4,2,256]{2,1,0:T(2,128)(2,1)S(1)} async-done(((bf16[4,2,256]{2,1,0:T(2,128)(2,1)}), bf16[4,2,256]{2,1,0:T(2,128)(2,1)S(1)}, u32[]{:S(2)}, u32[]{:S(2)}) %all-to-all-start.2) | async-done | bytes 4128 | tf_op jit(solution)/shard_map/all_to_all | solution.py:43
  49.9 3.2 %all-to-all-start = ((bf16[4,2,256]{2,1,0:T(2,128)(2,1)}), bf16[4,2,256]{2,1,0:T(2,128)(2,1)S(1)}, u32[]{:S(2)}, u32[]{:S(2)}) async-start(bf16[4,2,256]{2,1,0:T(2,128)(2,1)} %reshape.115), calls=%async_computation | async-start | bytes 8192 | tf_op jit(solution)/shard_map/all_to_all | solution.py:41
  53.1 0.1 reshape.118
  53.3 0.1 neg.75
  53.4 0.1 reshape.103
  53.4 5.2 %all-to-all-done = bf16[4,2,256]{2,1,0:T(2,128)(2,1)S(1)} async-done(((bf16[4,2,256]{2,1,0:T(2,128)(2,1)}), bf16[4,2,256]{2,1,0:T(2,128)(2,1)S(1)}, u32[]{:S(2)}, u32[]{:S(2)}) %all-to-all-start) | async-done | bytes 4128 | tf_op jit(solution)/shard_map/all_to_all | solution.py:41
  58.7 3.2 %all-to-all-start.3 = ((bf16[4,2,256]{2,1,0:T(2,128)(2,1)}), bf16[4,2,256]{2,1,0:T(2,128)(2,1)S(1)}, u32[]{:S(2)}, u32[]{:S(2)}) async-start(bf16[4,2,256]{2,1,0:T(2,128)(2,1)} %reshape.113), calls=%async_computation.3 | async-start | bytes 8192 | tf_op jit(solution)/shard_map/all_to_all | solution.py:44
  61.9 0.0 reduce-scatter.2.cloned.1.call-start
  62.0 0.1 reshape.116
  62.1 0.1 reshape.102
  62.2 0.1 fusion.23
  62.3 1.8 %multiply_add_fusion = f32[2,8,128,128]{3,2,1,0:T(8,128)S(1)} fusion(f32[2,8,128,128]{3,2,1,0:T(8,128)} %param.20, f32[2,8,128]{2,1,0:T(8,128)S(1)} %reshape.103, f32[2,8,128]{2,1,0:T(8,128)S(1)} %get-tuple-element.7, f32[2,8,128]{2,1,0:T(8,128)S(1)} %get-tuple-element.6), kind=kLoop, calls=%fused_computation.7 | loop fusion | flops 786432 | bytes 2121728 | tf_op jit(solution)/shard_map/add | solution.py:52
  64.1 0.0 copy-start.1
  64.1 1.0 fusion.25
  65.1 0.1 multiply_reduce_fusion
  65.2 2.3 %all-to-all-done.3 = bf16[4,2,256]{2,1,0:T(2,128)(2,1)S(1)} async-done(((bf16[4,2,256]{2,1,0:T(2,128)(2,1)}), bf16[4,2,256]{2,1,0:T(2,128)(2,1)S(1)}, u32[]{:S(2)}, u32[]{:S(2)}) %all-to-all-start.3) | async-done | bytes 4128 | tf_op jit(solution)/shard_map/all_to_all | solution.py:44
  67.5 0.1 reshape.114
  67.6 0.1 reshape.104
  67.7 0.1 multiply_convert_fusion
  67.8 1.8 %all_gather.13 = bf16[2,16,128]{2,1,0:T(8,128)(2,1)S(1)} all-gather(bf16[2,8,128]{2,1,0:T(8,128)(2,1)S(1)} %multiply_convert_fusion), channel_id=1, replica_groups=mesh['dp'=4,'kv'=4,'tp'=2] {'tp'}, dimensions={1}, use_global_device_ids=true | all-gather | bytes 12288 | tf_op jit(solution)/shard_map/all_gather | solution.py:61
  69.6 13.1 %all-gather = bf16[4,2,2048]{2,1,0:T(2,128)(2,1)S(1)} all-gather(bf16[1,2,2048]{2,1,0:T(2,128)(2,1)S(1)} %reshape.108), channel_id=1, replica_groups=mesh['dp'=4,'kv'=4,'tp'=2] {'kv'}, dimensions={0}, use_global_device_ids=true | all-gather | bytes 40960 | tf_op jit(solution)/shard_map/all_gather | solution.py:65
  82.8 0.4 fusion.2
  83.2 14.0 %all_gather.15 = bf16[8,4096]{1,0:T(8,128)(2,1)S(1)} all-gather(bf16[8,512]{1,0:T(8,128)(2,1)S(1)} %fusion.2), channel_id=1, replica_groups=mesh['dp'=4,'kv'=4,'tp'=2] {'kv','tp'}, dimensions={1}, use_global_device_ids=true | all-gather | bytes 73728 | tf_op jit(solution)/shard_map/all_gather | solution.py:10
  97.2 0.1 fusion.7
  97.3 0.0 copy-done.4
  97.3 13.5 %fusion.3 = f32[8,4096]{1,0:T(8,128)} fusion(bf16[2048,4096]{1,0:T(8,128)(2,1)} %param.25, bf16[4096,2048]{1,0:T(8,128)(2,1)} %param.24, bf16[8,4096]{1,0:T(8,128)(2,1)S(1)} %all_gather.15, f32[4096]{0:T(1024)S(1)} %copy-done.4, f32[8]{0:T(128)S(1)} %add_rsqrt_fusion.1), kind=kOutput, calls=%fused_computation.8 | convolution fusion | flops 268615680 | bytes 33767456 | tf_op jit(solution)/shard_map/dot_general | solution.py:77
  110.8 0.0 copy-done.1
  110.9 0.0 reduce-scatter.2.cloned.1.call-update
  110.9 29.9 %reduce-scatter.2.cloned.1.call-done = f32[8,512]{1,0:T(8,128)} async-done(((f32[8,4096]{1,0:T(8,128)}), f32[8,512]{1,0:T(8,128)}) %reduce-scatter.2.cloned.1.call-update) | async-done | bytes 16400 | tf_op jit(solution)/shard_map/reduce_scatter | solution.py:76
  140.7 1.3 add_convert_fusion
  (22 shorter events, 0.2 us)
Async XLA Ops:
  7.2 75.6 %copy-start = (bf16[16,128,512]{2,1,0:T(8,128)(2,1)S(1)}, bf16[16,128,512]{2,1,0:T(8,128)(2,1)}, u32[]{:S(2)}) copy-start(bf16[16,128,512]{2,1,0:T(8,128)(2,1)} %param.22) | copy-start | bytes 6291460
  23.4 4.4 %copy-start.3 = (f32[4096]{0:T(1024)S(1)}, f32[4096]{0:T(1024)}, u32[]{:S(2)}) copy-start(f32[4096]{0:T(1024)} %param.14) | copy-start | bytes 49156
  27.7 7.8 %copy-start.5 = (f32[8,128]{1,0:T(8,128)S(1)}, f32[8,128]{1,0:T(8,128)}, u32[]{:S(2)}) copy-start(f32[8,128]{1,0:T(8,128)} %param.19) | copy-start | bytes 12292
  27.8 39.9 %copy-start.6 = (f32[8,128]{1,0:T(8,128)S(1)}, f32[8,128]{1,0:T(8,128)}, u32[]{:S(2)}) copy-start(f32[8,128]{1,0:T(8,128)} %param.21) | copy-start | bytes 12292
  27.8 55.0 %copy-start.2 = (bf16[8,512]{1,0:T(8,128)(2,1)S(1)}, bf16[8,512]{1,0:T(8,128)(2,1)}, u32[]{:S(2)}) copy-start(bf16[8,512]{1,0:T(8,128)(2,1)} %param.13) | copy-start | bytes 24580
  27.8 69.5 %copy-start.4 = (f32[4096]{0:T(1024)S(1)}, f32[4096]{0:T(1024)}, u32[]{:S(2)}) copy-start(f32[4096]{0:T(1024)} %param.23) | copy-start | bytes 49156
  30.9 10.2 %all-to-all-start.1 = ((bf16[4,2,256]{2,1,0:T(2,128)(2,1)}), bf16[4,2,256]{2,1,0:T(2,128)(2,1)S(1)}, u32[]{:S(2)}, u32[]{:S(2)}) async-start(bf16[4,2,256]{2,1,0:T(2,128)(2,1)} %reshape.119), calls=%async_computation.1 | async-start | bytes 8192 | tf_op jit(solution)/shard_map/all_to_all | solution.py:42
  41.1 8.8 %all-to-all-start.2 = ((bf16[4,2,256]{2,1,0:T(2,128)(2,1)}), bf16[4,2,256]{2,1,0:T(2,128)(2,1)S(1)}, u32[]{:S(2)}, u32[]{:S(2)}) async-start(bf16[4,2,256]{2,1,0:T(2,128)(2,1)} %reshape.117), calls=%async_computation.2 | async-start | bytes 8192 | tf_op jit(solution)/shard_map/all_to_all | solution.py:43
  49.9 8.8 %all-to-all-start = ((bf16[4,2,256]{2,1,0:T(2,128)(2,1)}), bf16[4,2,256]{2,1,0:T(2,128)(2,1)S(1)}, u32[]{:S(2)}, u32[]{:S(2)}) async-start(bf16[4,2,256]{2,1,0:T(2,128)(2,1)} %reshape.115), calls=%async_computation | async-start | bytes 8192 | tf_op jit(solution)/shard_map/all_to_all | solution.py:41
  58.7 8.8 %all-to-all-start.3 = ((bf16[4,2,256]{2,1,0:T(2,128)(2,1)}), bf16[4,2,256]{2,1,0:T(2,128)(2,1)S(1)}, u32[]{:S(2)}, u32[]{:S(2)}) async-start(bf16[4,2,256]{2,1,0:T(2,128)(2,1)} %reshape.113), calls=%async_computation.3 | async-start | bytes 8192 | tf_op jit(solution)/shard_map/all_to_all | solution.py:44
  61.9 78.8 %reduce-scatter.2.cloned.1.call-start = ((), (), s32[]{:S(2)}) async-start(), calls=%async_computation.5 | async-start | bytes 147456 | tf_op jit(solution)/shard_map/reduce_scatter | solution.py:76
  64.1 46.7 %copy-start.1 = (f32[2,8,128,128]{3,2,1,0:T(8,128)}, f32[2,8,128,128]{3,2,1,0:T(8,128)S(1)}, u32[]{:S(2)}) copy-start(f32[2,8,128,128]{3,2,1,0:T(8,128)S(1)} %multiply_add_fusion) | copy-start | bytes 3145732
Sparse Core Ops, SparseCore 0:
  111.0 29.6 reduce-scatter.1
where the time goes:
time: 149 us
  waiting for transfers between devices  46.4 us (31%)
  blocking collectives  45 us (30%)
  matrix products  17.1 us (11%)
  starting transfers between devices  14.4 us (10%)
  between operations  14.2 us (10%)
  other arithmetic  8.09 us (5%)
  local copies, waits for them, and re-layouts  3.68 us (2%)
    all_gather x2, blocking collectives, normed_rows(): lax.all_gather(row_block, ('kv', 'tp'), axis=1, tiled=True)  30 us
    reduce_scatter x1, waiting for transfers between devices, local(): lax.psum_scatter(jnp.dot(hidden, down_weight, preferred_element_type=jnp....  29.9 us
    dot_general x1, matrix products, local(): jnp.dot(hidden, down_weight, preferred_element_type=jnp.float32)  13.5 us
    all_gather x1, blocking collectives, local(): lax.all_gather(flat_mixed, 'kv', axis=0, tiled=True)  13.1 us
    all_to_all x1, waiting for transfers between devices, local(): lax.all_to_all(product[:, 2], 'kv', split_axis=0, concat_axis=2, tiled=True)  5.45 us
    all_to_all x1, waiting for transfers between devices, local(): lax.all_to_all(product[:, 0], 'kv', split_axis=0, concat_axis=2, tiled=True)  5.25 us
    all_to_all x1, starting transfers between devices, local(): lax.all_to_all(product[:, 1], 'kv', split_axis=0, concat_axis=2, tiled=True)  4.64 us
    another operation x1, other arithmetic, local(): jnp.stack((query_weight, forget_weight, value_weight, gate_weight), axis=0)  4.36 us
  transfers between devices with their start and end apart: 5, of which 5 were waited for; matrix products, arithmetic and copies ran while one was open for 4% of the time, Pallas kernels for 0%

commit v1 on v0

--- a/solution.py
+++ b/solution.py
@@ -1,9 +1,15 @@
+import functools
+
 import jax
 import jax.numpy as jnp
 from jax import lax
+from jax.experimental import pallas as pl
+from jax.experimental.pallas import tpu as pltpu
 from jax.sharding import PartitionSpec as P
 
 epsilon = 1e-06
+VMEM_LIMIT = 67043328
+MESH = pl.DeviceIdType.MESH
 
 
 def normed_rows(row_block, gain_vector):
@@ -13,7 +19,7 @@
     return result_rows
 
 
-def local(
+def local_plain(
     tokens,
     mix_gain,
     query_weight,
@@ -83,6 +89,314 @@
     return (layer_output, next_state)
 
 
+def sigmoid(x):
+    return 1.0 / (1.0 + jnp.exp(-x))
+
+
+def kernel(
+    KV, TP, LH, UP_CHUNKS, DOWN_CHUNKS,
+    tok_h, mixg_h, qw_h, fw_h, vw_h, gw_h, lb_h, st_h, hg_h, ow_h, mlpg_h, uw_h, dw_h,
+    out_h, ns_h,
+    xsrc, mixg, lb, hg, mlpg, wbuf, stbuf, nsbuf, obuf, ubuf, dbuf, outbuf,
+    xbuf, asend, arecv, heads, msend, mrecv, rsend, rbuf, psend, pbuf, xn, hid,
+    local_sem, up_sem, down_sem, send_sem, recv_sem,
+):
+    N = KV * TP
+    kv, tp = lax.axis_index("kv"), lax.axis_index("tp")
+    me = kv * TP + tp
+    nb, block = xsrc.shape
+    per = stbuf.shape[0] // LH
+    lane = stbuf.shape[2]
+    lc = wbuf.shape[1] // LH
+
+    small = [
+        pltpu.make_async_copy(src, dst, local_sem.at[i])
+        for i, (src, dst) in enumerate(
+            ((tok_h, xsrc), (mixg_h, mixg), (lb_h, lb), (hg_h, hg), (mlpg_h, mlpg))
+        )
+    ]
+    weights = [
+        pltpu.make_async_copy(src, wbuf.at[i], local_sem.at[5 + i])
+        for i, src in enumerate((qw_h, fw_h, vw_h, gw_h))
+    ]
+    state_in = pltpu.make_async_copy(st_h, stbuf, local_sem.at[9])
+    out_in = pltpu.make_async_copy(ow_h, obuf, local_sem.at[10])
+    uk = ubuf.shape[0] // UP_CHUNKS
+    ups = [
+        pltpu.make_async_copy(
+            uw_h.at[pl.ds(i * uk, uk)], ubuf.at[pl.ds(i * uk, uk)], up_sem.at[i]
+        )
+        for i in range(UP_CHUNKS)
+    ]
+    dk = dbuf.shape[0] // DOWN_CHUNKS
+    downs = [
+        pltpu.make_async_copy(
+            dw_h.at[pl.ds(i * dk, dk)], dbuf.at[pl.ds(i * dk, dk)], down_sem.at[i]
+        )
+        for i in range(DOWN_CHUNKS)
+    ]
+    for copy in small + weights + [state_in, out_in] + ups + downs:
+        copy.start()
+
+    def where(index):
+        return {"kv": index // TP, "tp": lax.rem(index, TP)}
+
+    barrier = pltpu.get_barrier_semaphore()
+    for o in range(1, N):
+        pl.semaphore_signal(
+            barrier, inc=1, device_id=where(lax.rem(me + o, N)), device_id_type=MESH
+        )
+    pl.semaphore_wait(barrier, N - 1)
+
+    def push(phase, src, dst, o, peer):
+        copy = pltpu.make_async_remote_copy(
+            src_ref=src,
+            dst_ref=dst,
+            send_sem=send_sem.at[phase, o],
+            recv_sem=recv_sem.at[phase, me],
+            device_id=where(peer),
+            device_id_type=MESH,
+        )
+        copy.start()
+        return copy
+
+    def take(phase, src, dst, peer):
+        pltpu.make_async_remote_copy(
+            src_ref=src,
+            dst_ref=dst,
+            send_sem=send_sem.at[phase, 0],
+            recv_sem=recv_sem.at[phase, peer],
+            device_id=where(peer),
+            device_id_type=MESH,
+        ).wait_recv()
+
+    sent = []
+
+    def gather(phase, src, buf):
+        for o in range(1, N):
+            sent.append(push(phase, src, buf.at[me], o, lax.rem(me + o, N)))
+        buf[me] = src[...]
+        for o in range(1, N):
+            peer = lax.rem(me + o, N)
+            take(phase, src, buf.at[peer], peer)
+
+    def norm_into(buf, gain):
+        total = jnp.zeros((nb, 1), jnp.float32)
+        for j in range(N):
+            piece = buf[j].astype(jnp.float32)
+            total = total + jnp.sum(piece * piece, axis=1, keepdims=True)
+        inv = lax.rsqrt(total / (N * block) + epsilon)
+        for j in range(N):
+            cols = slice(j * block, (j + 1) * block)
+            piece = buf[j].astype(jnp.float32)
+            xn[:, cols] = (piece * inv * gain[:, cols]).astype(jnp.bfloat16)
+
+    small[0].wait()
+    gather(0, xsrc, xbuf)
+    small[1].wait()
+    norm_into(xbuf, mixg)
+
+    for w in range(4):
+        weights[w].wait()
+        prod = lax.dot_general(
+            xn[...], wbuf[w], (((1,), (1,)), ((), ())), preferred_element_type=jnp.float32
+        )
+        prod = prod.astype(jnp.bfloat16).astype(jnp.float32)
+        for j in range(KV):
+            asend[j, w * per : (w + 1) * per, :] = prod[j * per : (j + 1) * per, :]
+    for o in range(1, KV):
+        other = lax.rem(kv + o, KV)
+        sent.append(push(1, asend.at[other], arecv.at[kv], o, other * TP + tp))
+    arecv[kv] = asend[kv]
+    for copy in small[2:]:
+        copy.wait()
+    for o in range(1, KV):
+        other = lax.rem(kv + o, KV)
+        take(1, asend.at[other], arecv.at[other], other * TP + tp)
+    for h in range(LH):
+        row = jnp.concatenate(
+            [arecv[s, :, h * lc : (h + 1) * lc] for s in range(KV)], axis=1
+        )
+        for i in range(4 * per):
+            heads[i, h : h + 1, :] = row[i : i + 1, :]
+
+    def kind(w):
+        return heads[w * per : (w + 1) * per].reshape(per * LH, lane)
+
+    low = jnp.concatenate([lb[...]] * per, axis=0)
+    pre_q, pre_f, val, gate = kind(0), kind(1), kind(2), kind(3)
+    forget = low + (1.0 - low) * sigmoid(pre_f)
+    key = (1.0 - low) * sigmoid(-pre_f)
+    query = pre_q * sigmoid(pre_q)
+    items = per * LH
+    stacked = jnp.concatenate(
+        [forget, key, query, jnp.zeros((lane - 3 * items, lane), jnp.float32)], axis=0
+    )
+    cols = stacked.T
+    state_in.wait()
+    rows = []
+    for i in range(items):
+        new = (
+            cols[:, i : i + 1] * stbuf[i]
+            + cols[:, items + i : items + i + 1] * val[i : i + 1, :]
+        )
+        nsbuf[i] = new
+        rows.append(
+            jnp.sum(cols[:, 2 * items + i : 2 * items + i + 1] * new, axis=0, keepdims=True)
+        )
+    readout = jnp.concatenate(rows, axis=0)
+    state_out = pltpu.make_async_copy(nsbuf, ns_h, local_sem.at[11])
+    state_out.start()
+    inv_head = lax.rsqrt(jnp.mean(readout * readout, axis=1, keepdims=True) + epsilon)
+    gains = jnp.concatenate([hg[...]] * per, axis=0)
+    mixed = readout * inv_head * gains * (gate * sigmoid(gate))
+    for r in range(per):
+        for h in range(LH):
+            msend[r : r + 1, h * lane : (h + 1) * lane] = mixed[r * LH + h : r * LH + h + 1, :]
+    gather(2, msend, mrecv)
+    flat = jnp.concatenate(
+        [
+            jnp.concatenate([mrecv[s * TP + t] for s in range(KV)], axis=0)
+            for t in range(TP)
+        ],
+        axis=1,
+    ).astype(jnp.bfloat16)
+
+    out_in.wait()
+    projected = jnp.dot(flat, obuf[...], preferred_element_type=jnp.float32)
+    rsend[...] = (xsrc[...].astype(jnp.float32) + projected).astype(jnp.bfloat16)
+    gather(3, rsend, rbuf)
+    norm_into(rbuf, mlpg)
+
+    for copy in ups:
+        copy.wait()
+    tile = min(512, ubuf.shape[1])
+
+    @pl.loop(0, ubuf.shape[1] // tile)
+    def _(n):
+        at = pl.ds(pl.multiple_of(n * tile, tile), tile)
+        act = jnp.maximum(jnp.dot(xn[...], ubuf[:, at], preferred_element_type=jnp.float32), 0.0)
+        hid[:, at] = (act * act).astype(jnp.bfloat16)
+
+    for copy in downs:
+        copy.wait()
+
+    def partial_sum(peer):
+        at = pl.ds(pl.multiple_of(peer * block, block), block)
+        return jnp.dot(hid[...], dbuf[:, at], preferred_element_type=jnp.float32)
+
+    @pl.loop(1, N)
+    def _(o):
+        peer = lax.rem(me + o, N)
+        psend[o] = partial_sum(peer)
+        push(4, psend.at[o], pbuf.at[me], o, peer)
+
+    pbuf[me] = partial_sum(me)
+    for o in range(1, N):
+        peer = lax.rem(me + o, N)
+        take(4, psend.at[0], pbuf.at[peer], peer)
+    summed = pbuf[0]
+    for j in range(1, N):
+        summed = summed + pbuf[j]
+    outbuf[...] = (rsend[...].astype(jnp.float32) + summed).astype(jnp.bfloat16)
+    last = pltpu.make_async_copy(outbuf, out_h, local_sem.at[0])
+    last.start()
+    for copy in sent:
+        copy.wait_send()
+    for o in range(1, N):
+        pltpu.make_async_remote_copy(
+            src_ref=psend.at[o],
+            dst_ref=pbuf.at[me],
+            send_sem=send_sem.at[4, o],
+            recv_sem=recv_sem.at[4, me],
+            device_id=where(lax.rem(me + o, N)),
+            device_id_type=MESH,
+        ).wait_send()
+    last.wait()
+    state_out.wait()
+
+
+def local_kernel(KV, TP, *args):
+    (tokens, mix_gain, qw, fw, vw, gw, lower_bound, state, head_gain, ow, mlp_gain, uw, dw) = args
+    nb, block = tokens.shape
+    LH, lc, D = qw.shape
+    per, _, kd, vd = state.shape
+    N = KV * TP
+    UP, DOWN = 8, 8
+    bf, f32 = jnp.bfloat16, jnp.float32
+    flat = lambda a: a.reshape(-1, a.shape[-1])
+    hidden = uw.shape[1]
+    out, ns = pl.pallas_call(
+        functools.partial(kernel, KV, TP, LH, UP, DOWN),
+        out_shape=(
+            jax.ShapeDtypeStruct((nb, block), bf),
+            jax.ShapeDtypeStruct((per * LH, kd, vd), f32),
+        ),
+        in_specs=[pl.BlockSpec(memory_space=pl.ANY)] * 13,
+        out_specs=(pl.BlockSpec(memory_space=pl.ANY),) * 2,
+        scratch_shapes=[
+            pltpu.VMEM((nb, block), bf),
+            pltpu.VMEM((1, D), f32),
+            pltpu.VMEM((LH, kd), f32),
+            pltpu.VMEM((LH, vd), f32),
+            pltpu.VMEM((1, D), f32),
+            pltpu.VMEM((4, LH * lc, D), bf),
+            pltpu.VMEM((per * LH, kd, vd), f32),
+            pltpu.VMEM((per * LH, kd, vd), f32),
+            pltpu.VMEM((ow.shape[0] * ow.shape[1], block), bf),
+            pltpu.VMEM(uw.shape, bf),
+            pltpu.VMEM(dw.shape, bf),
+            pltpu.VMEM((nb, block), bf),
+            pltpu.VMEM((N, nb, block), bf),
+            pltpu.VMEM((KV, 4 * per, LH * lc), f32),
+            pltpu.VMEM((KV, 4 * per, LH * lc), f32),
+            pltpu.VMEM((4 * per, LH, kd), f32),
+            pltpu.VMEM((per, LH * vd), f32),
+            pltpu.VMEM((N, per, LH * vd), f32),
+            pltpu.VMEM((nb, block), bf),
+            pltpu.VMEM((N, nb, block), bf),
+            pltpu.VMEM((N, nb, block), f32),
+            pltpu.VMEM((N, nb, block), f32),
+            pltpu.VMEM((nb, D), bf),
+            pltpu.VMEM((nb, hidden), bf),
+            pltpu.SemaphoreType.DMA((12,)),
+            pltpu.SemaphoreType.DMA((UP,)),
+            pltpu.SemaphoreType.DMA((DOWN,)),
+            pltpu.SemaphoreType.DMA((5, N)),
+            pltpu.SemaphoreType.DMA((5, N)),
+        ],
+        compiler_params=pltpu.CompilerParams(
+            collective_id=0, has_side_effects=True, vmem_limit_bytes=VMEM_LIMIT
+        ),
+    )(
+        tokens, mix_gain.reshape(1, -1), flat(qw), flat(fw), flat(vw), flat(gw), lower_bound,
+        state.reshape(-1, kd, vd), head_gain, flat(ow), mlp_gain.reshape(1, -1), uw, dw,
+    )
+    return out, ns.reshape(state.shape)
+
+
+def local(KV, TP, *args):
+    tokens, qw, state = args[0], args[2], args[7]
+    nb, block = tokens.shape
+    LH, lc, _ = qw.shape
+    per, _, kd, vd = state.shape
+    fits = (
+        block % 128 == 0
+        and (LH * lc) % 128 == 0
+        and kd == 128
+        and vd == 128
+        and nb % 8 == 0
+        and (4 * per) % 8 == 0
+        and LH % 8 == 0
+        and 3 * per * LH <= kd
+        and args[11].shape[1] % 512 == 0
+        and KV > 1
+    )
+    if fits:
+        return local_kernel(KV, TP, *args)
+    return local_plain(*args)
+
+
 def solution(mesh):
     placed = (
         P("dp", ("kv", "tp")),
@@ -100,7 +414,7 @@
         P(("kv", "tp"), None),
     )
     return jax.shard_map(
-        local,
+        functools.partial(local, mesh.shape["kv"], mesh.shape["tp"]),
         mesh=mesh,
         in_specs=placed,
         out_specs=(P("dp", ("kv", "tp")), P(("dp", "kv"), "tp", None, None)),

time: 149 us -> 40.4 us (0.27)
  waiting for transfers between devices: 46.4 us -> 0 us
  blocking collectives: 45 us -> 0 us
  Pallas kernels: 0 us -> 35.9 us
  matrix products: 17.1 us -> 0 us
  starting transfers between devices: 14.4 us -> 0 us
  between operations: 14.2 us -> 0.64 us
  other arithmetic: 8.09 us -> 0 us
    all_gather x4 -> x0, blocking collectives: 45 us -> none  [the longest x2 30 us: normed_rows(): lax.all_gather(row_block, ('kv', 'tp'), axis=1, tiled=True)]
    pallas_call x0 -> x1, Pallas kernels: none -> 35.9 us  [local_kernel(): pl.pallas_call(functools.partial(kernel, KV, TP, LH, UP, DOWN), out_shape...]
    reduce_scatter x1 -> x0, waiting for transfers between devices: 29.9 us -> none  [local(): lax.psum_scatter(jnp.dot(hidden, down_weight, preferred_element_type=jnp....]
    dot_general x4 -> x0, matrix products: 17.1 us -> none  [the longest x1 13.5 us: local(): jnp.dot(hidden, down_weight, preferred_element_type=jnp.float32)]
    all_to_all x4 -> x0, waiting for transfers between devices: 16.5 us -> none  [the longest x1 5.45 us: local(): lax.all_to_all(product[:, 2], 'kv', split_axis=0, concat_axis=2, tiled=True)]
    all_to_all x4 -> x0, starting transfers between devices: 14.4 us -> none  [the longest x1 4.64 us: local(): lax.all_to_all(product[:, 1], 'kv', split_axis=0, concat_axis=2, tiled=True)]
    another operation x1 -> x0, other arithmetic: 4.36 us -> none  [local(): jnp.stack((query_weight, forget_weight, value_weight, gate_weight), axis=0)]
    add x1 -> x0, other arithmetic: 1.83 us -> none  [local(): jnp.exp(log_forget)[:, :, :, None] * recurrent_state]
  transfers between devices with their start and end apart: 5 -> 0, of which waited for: 5 -> 0; matrix products, arithmetic and copies ran while one was open for 4% -> 0% of each run, Pallas kernels for 0% -> 0%
where the time goes in v1:
time: 40.4 us; the launch traced here: 40.2 us
  Pallas kernels  35.9 us (89%)
  local copies, waits for them, and re-layouts  3.59 us (9%)
  between operations  0.64 us (2%)
    pallas_call x1, Pallas kernels, local_kernel(): pl.pallas_call(functools.partial(kernel, KV, TP, LH, UP, DOWN), out_shape...  35.9 us
    unnamed x2, local copies, waits for them, and re-layouts  3.59 us

profile of v1, /device:TPU:0, one launch (start us, length us, event | category | flops | bytes accessed | tf_op | source)
XLA Modules:
  0.0 40.2 jit_solution(2835291650632642891)
XLA Ops:
  0.6 35.9 %shard_map.140 = (bf16[8,512]{1,0:T(8,128)(2,1)}, f32[16,128,128]{2,1,0:T(8,128)}) custom-call(bf16[8,512]{1,0:T(8,128)(2,1)} %tok_h.1, f32[1,4096]{1,0:T(1,128)} %bitcast.16, bf16[256,4096]{1,0:T(8,128)(2,1)} %bitcast.9, bf16[256,4096]{1,0:T(8,128)(2,1)} %bitcast.10, bf16[256,4096]{1,0:T(8,128)(2,1)} %bitcast.11, bf16[256,4096]{1,0:T(8,128)(2,1)} %bitcast.12, ...), custom_call_target="tpu_custom_call" | custom-call | tf_op jit(solution)/shard_map/pallas_call | solution.py:329
  36.6 1.3 %copy.17 = bf16[8,512]{1,0:T(8,128)(2,1)} copy(bf16[8,512]{1,0:T(8,128)(2,1)} %get-tuple-element.8) | data formatting | bytes 16384
  37.9 2.3 %copy.18 = f32[2,8,128,128]{3,2,1,0:T(8,128)} copy(f32[2,8,128,128]{3,2,1,0:T(8,128)} %bitcast.15) | data formatting | bytes 2097152

commit v2 on v1

--- a/solution.py
+++ b/solution.py
@@ -98,7 +98,7 @@
     tok_h, mixg_h, qw_h, fw_h, vw_h, gw_h, lb_h, st_h, hg_h, ow_h, mlpg_h, uw_h, dw_h,
     out_h, ns_h,
     xsrc, mixg, lb, hg, mlpg, wbuf, stbuf, nsbuf, obuf, ubuf, dbuf, outbuf,
-    xbuf, asend, arecv, heads, msend, mrecv, rsend, rbuf, psend, pbuf, xn, hid,
+    xbuf, asend, arecv, heads, mrow, msend, mrecv, rsend, rbuf, psend, pbuf, acc, hid,
     local_sem, up_sem, down_sem, send_sem, recv_sem,
 ):
     N = KV * TP
@@ -135,7 +135,7 @@
         )
         for i in range(DOWN_CHUNKS)
     ]
-    for copy in small + weights + [state_in, out_in] + ups + downs:
+    for copy in small + weights:
         copy.start()
 
     def where(index):
@@ -146,7 +146,20 @@
         pl.semaphore_signal(
             barrier, inc=1, device_id=where(lax.rem(me + o, N)), device_id_type=MESH
         )
+    for copy in [state_in, out_in] + ups:
+        copy.start()
     pl.semaphore_wait(barrier, N - 1)
+
+    def flip(index, mask):
+        bit = 1
+        result = index
+        while bit <= mask:
+            if mask & bit:
+                result = result + bit - 2 * bit * lax.rem(index // bit, 2)
+            bit *= 2
+        return result
+
+    order = [flip(kv, m // TP) * TP + lax.rem(tp + m, TP) for m in range(N)]
 
     def push(phase, src, dst, o, peer):
         copy = pltpu.make_async_remote_copy(
@@ -172,51 +185,63 @@
 
     sent = []
 
-    def gather(phase, src, buf):
-        for o in range(1, N):
-            sent.append(push(phase, src, buf.at[me], o, lax.rem(me + o, N)))
+    def spread(phase, src, buf):
+        for o in reversed(range(1, N)):
+            sent.append(push(phase, src, buf.at[me], o, order[o]))
         buf[me] = src[...]
-        for o in range(1, N):
-            peer = lax.rem(me + o, N)
-            take(phase, src, buf.at[peer], peer)
-
-    def norm_into(buf, gain):
-        total = jnp.zeros((nb, 1), jnp.float32)
-        for j in range(N):
-            piece = buf[j].astype(jnp.float32)
-            total = total + jnp.sum(piece * piece, axis=1, keepdims=True)
-        inv = lax.rsqrt(total / (N * block) + epsilon)
-        for j in range(N):
-            cols = slice(j * block, (j + 1) * block)
-            piece = buf[j].astype(jnp.float32)
-            xn[:, cols] = (piece * inv * gain[:, cols]).astype(jnp.bfloat16)
+
+    def columns(peer):
+        return pl.ds(pl.multiple_of(peer * block, block), block)
+
+    def scaled(piece, gain, at, total):
+        piece = piece.astype(jnp.float32)
+        total = total + jnp.sum(piece * piece, axis=1, keepdims=True)
+        return (piece * gain[:, at]).astype(jnp.bfloat16), total
+
+    def inverse(total):
+        return lax.rsqrt(total / (N * block) + epsilon)
 
     small[0].wait()
-    gather(0, xsrc, xbuf)
+    spread(0, xsrc, xbuf)
     small[1].wait()
-    norm_into(xbuf, mixg)
-
-    for w in range(4):
-        weights[w].wait()
-        prod = lax.dot_general(
-            xn[...], wbuf[w], (((1,), (1,)), ((), ())), preferred_element_type=jnp.float32
-        )
-        prod = prod.astype(jnp.bfloat16).astype(jnp.float32)
-        for j in range(KV):
-            asend[j, w * per : (w + 1) * per, :] = prod[j * per : (j + 1) * per, :]
-    for o in range(1, KV):
-        other = lax.rem(kv + o, KV)
+    for copy in weights:
+        copy.wait()
+    for copy in downs:
+        copy.start()
+    total = jnp.zeros((nb, 1), jnp.float32)
+    prods = [jnp.zeros((nb, wbuf.shape[1]), jnp.float32)] * 4
+    for o in range(N):
+        peer = order[o]
+        if o:
+            take(0, xsrc, xbuf.at[peer], peer)
+        at = columns(peer)
+        piece, total = scaled(xbuf[peer], mixg, at, total)
+        for w in range(4):
+            prods[w] = prods[w] + lax.dot_general(
+                piece,
+                wbuf[w, :, at],
+                (((1,), (1,)), ((), ())),
+                preferred_element_type=jnp.float32,
+            )
+    inv = inverse(total)
+    prods = [(prod * inv).astype(jnp.bfloat16).astype(jnp.float32) for prod in prods]
+
+    for j in range(KV):
+        asend[j] = jnp.concatenate(
+            [prod[j * per : (j + 1) * per, :] for prod in prods], axis=0
+        ).astype(jnp.bfloat16)
+    for o in reversed(range(1, KV)):
+        other = flip(kv, o)
         sent.append(push(1, asend.at[other], arecv.at[kv], o, other * TP + tp))
     arecv[kv] = asend[kv]
     for copy in small[2:]:
         copy.wait()
     for o in range(1, KV):
-        other = lax.rem(kv + o, KV)
+        other = flip(kv, o)
         take(1, asend.at[other], arecv.at[other], other * TP + tp)
+    parts = [arecv[s].astype(jnp.float32) for s in range(KV)]
     for h in range(LH):
-        row = jnp.concatenate(
-            [arecv[s, :, h * lc : (h + 1) * lc] for s in range(KV)], axis=1
-        )
+        row = jnp.concatenate([part[:, h * lc : (h + 1) * lc] for part in parts], axis=1)
         for i in range(4 * per):
             heads[i, h : h + 1, :] = row[i : i + 1, :]
 
@@ -252,11 +277,16 @@
     mixed = readout * inv_head * gains * (gate * sigmoid(gate))
     for r in range(per):
         for h in range(LH):
-            msend[r : r + 1, h * lane : (h + 1) * lane] = mixed[r * LH + h : r * LH + h + 1, :]
-    gather(2, msend, mrecv)
+            mrow[r : r + 1, h * lane : (h + 1) * lane] = mixed[r * LH + h : r * LH + h + 1, :]
+    msend[...] = mrow[...].astype(jnp.bfloat16)
+    spread(2, msend, mrecv)
+    for o in range(1, N):
+        take(2, msend, mrecv.at[order[o]], order[o])
     flat = jnp.concatenate(
         [
-            jnp.concatenate([mrecv[s * TP + t] for s in range(KV)], axis=0)
+            jnp.concatenate(
+                [mrecv[s * TP + t].astype(jnp.float32) for s in range(KV)], axis=0
+            )
             for t in range(TP)
         ],
         axis=1,
@@ -265,53 +295,43 @@
     out_in.wait()
     projected = jnp.dot(flat, obuf[...], preferred_element_type=jnp.float32)
     rsend[...] = (xsrc[...].astype(jnp.float32) + projected).astype(jnp.bfloat16)
-    gather(3, rsend, rbuf)
-    norm_into(rbuf, mlpg)
+    spread(3, rsend, rbuf)
 
     for copy in ups:
         copy.wait()
     tile = min(512, ubuf.shape[1])
-
-    @pl.loop(0, ubuf.shape[1] // tile)
-    def _(n):
-        at = pl.ds(pl.multiple_of(n * tile, tile), tile)
-        act = jnp.maximum(jnp.dot(xn[...], ubuf[:, at], preferred_element_type=jnp.float32), 0.0)
-        hid[:, at] = (act * act).astype(jnp.bfloat16)
+    total = jnp.zeros((nb, 1), jnp.float32)
+    for o in range(N):
+        peer = order[o]
+        if o:
+            take(3, rsend, rbuf.at[peer], peer)
+        at = columns(peer)
+        piece, total = scaled(rbuf[peer], mlpg, at, total)
+        for n in range(ubuf.shape[1] // tile):
+            to = slice(n * tile, (n + 1) * tile)
+            term = jnp.dot(piece, ubuf[at, to], preferred_element_type=jnp.float32)
+            acc[:, to] = term if o == 0 else acc[:, to] + term
+    act = jnp.maximum(acc[...] * inverse(total), 0.0)
+    hid[...] = (act * act).astype(jnp.bfloat16)
 
     for copy in downs:
         copy.wait()
 
     def partial_sum(peer):
-        at = pl.ds(pl.multiple_of(peer * block, block), block)
-        return jnp.dot(hid[...], dbuf[:, at], preferred_element_type=jnp.float32)
-
-    @pl.loop(1, N)
-    def _(o):
-        peer = lax.rem(me + o, N)
-        psend[o] = partial_sum(peer)
-        push(4, psend.at[o], pbuf.at[me], o, peer)
-
-    pbuf[me] = partial_sum(me)
+        return jnp.dot(hid[...], dbuf[:, columns(peer)], preferred_element_type=jnp.float32)
+
+    for o in reversed(range(1, N)):
+        psend[o] = partial_sum(order[o]).astype(jnp.bfloat16)
+        sent.append(push(4, psend.at[o], pbuf.at[me], o, order[o]))
+    summed = partial_sum(me)
     for o in range(1, N):
-        peer = lax.rem(me + o, N)
-        take(4, psend.at[0], pbuf.at[peer], peer)
-    summed = pbuf[0]
-    for j in range(1, N):
-        summed = summed + pbuf[j]
+        take(4, psend.at[0], pbuf.at[order[o]], order[o])
+        summed = summed + pbuf[order[o]].astype(jnp.float32)
     outbuf[...] = (rsend[...].astype(jnp.float32) + summed).astype(jnp.bfloat16)
     last = pltpu.make_async_copy(outbuf, out_h, local_sem.at[0])
     last.start()
     for copy in sent:
         copy.wait_send()
-    for o in range(1, N):
-        pltpu.make_async_remote_copy(
-            src_ref=psend.at[o],
-            dst_ref=pbuf.at[me],
-            send_sem=send_sem.at[4, o],
-            recv_sem=recv_sem.at[4, me],
-            device_id=where(lax.rem(me + o, N)),
-            device_id_type=MESH,
-        ).wait_send()
     last.wait()
     state_out.wait()
 
@@ -348,16 +368,17 @@
             pltpu.VMEM(dw.shape, bf),
             pltpu.VMEM((nb, block), bf),
             pltpu.VMEM((N, nb, block), bf),
-            pltpu.VMEM((KV, 4 * per, LH * lc), f32),
-            pltpu.VMEM((KV, 4 * per, LH * lc), f32),
+            pltpu.VMEM((KV, 4 * per, LH * lc), bf),
+            pltpu.VMEM((KV, 4 * per, LH * lc), bf),
             pltpu.VMEM((4 * per, LH, kd), f32),
             pltpu.VMEM((per, LH * vd), f32),
-            pltpu.VMEM((N, per, LH * vd), f32),
+            pltpu.VMEM((per, LH * vd), bf),
+            pltpu.VMEM((N, per, LH * vd), bf),
             pltpu.VMEM((nb, block), bf),
             pltpu.VMEM((N, nb, block), bf),
-            pltpu.VMEM((N, nb, block), f32),
-            pltpu.VMEM((N, nb, block), f32),
-            pltpu.VMEM((nb, D), bf),
+            pltpu.VMEM((N, nb, block), bf),
+            pltpu.VMEM((N, nb, block), bf),
+            pltpu.VMEM((nb, hidden), f32),
             pltpu.VMEM((nb, hidden), bf),
             pltpu.SemaphoreType.DMA((12,)),
             pltpu.SemaphoreType.DMA((UP,)),
@@ -391,6 +412,7 @@
         and 3 * per * LH <= kd
         and args[11].shape[1] % 512 == 0
         and KV > 1
+        and KV & (KV - 1) == 0
     )
     if fits:
         return local_kernel(KV, TP, *args)

time: 40.4 us -> 34.2 us (0.85)
  Pallas kernels: 35.9 us -> 29.8 us
    pallas_call x1, Pallas kernels: 35.9 us -> 29.8 us  [local_kernel(): pl.pallas_call(functools.partial(kernel, KV, TP, LH, UP, DOWN), out_shape...]
where the time goes in v2:
time: 34.2 us; the launch traced here: 34 us
  Pallas kernels  29.8 us (87%)
  local copies, waits for them, and re-layouts  3.59 us (10%)
  between operations  0.64 us (2%)
    pallas_call x1, Pallas kernels, local_kernel(): pl.pallas_call(functools.partial(kernel, KV, TP, LH, UP, DOWN), out_shape...  29.8 us
    unnamed x2, local copies, waits for them, and re-layouts  3.59 us

profile of v2, /device:TPU:0, one launch (start us, length us, event | category | flops | bytes accessed | tf_op | source)
XLA Modules:
  0.0 34.0 jit_solution(6775088753937580701)
XLA Ops:
  0.6 29.8 %shard_map.140 = (bf16[8,512]{1,0:T(8,128)(2,1)}, f32[16,128,128]{2,1,0:T(8,128)}) custom-call(bf16[8,512]{1,0:T(8,128)(2,1)} %tok_h.1, f32[1,4096]{1,0:T(1,128)} %bitcast.16, bf16[256,4096]{1,0:T(8,128)(2,1)} %bitcast.9, bf16[256,4096]{1,0:T(8,128)(2,1)} %bitcast.10, bf16[256,4096]{1,0:T(8,128)(2,1)} %bitcast.11, bf16[256,4096]{1,0:T(8,128)(2,1)} %bitcast.12, ...), custom_call_target="tpu_custom_call" | custom-call | tf_op jit(solution)/shard_map/pallas_call | solution.py:349
  30.4 1.3 %copy.17 = bf16[8,512]{1,0:T(8,128)(2,1)} copy(bf16[8,512]{1,0:T(8,128)(2,1)} %get-tuple-element.8) | data formatting | bytes 16384
  31.7 2.3 %copy.18 = f32[2,8,128,128]{3,2,1,0:T(8,128)} copy(f32[2,8,128,128]{3,2,1,0:T(8,128)} %bitcast.15) | data formatting | bytes 2097152
